TPU v7x, 32 devices: a whole 2x2x4 slice. The times are simulated.
32 devices in a mesh: ep: 8 (over z, core), tp: 4 (over y, x).
Axes of the slice: x: 2, y: 2, z: 4, core: 2. Of those that a mesh axis runs over, the one named last changes fastest.
Arguments:
- branch_in: bfloat16 [8192, 512], P(('ep', 'tp')), may hold values from -6 to 6
- pool_weight: bfloat16 [4, 128, 128], replicated, may hold values from -0.5 to 0.5
- group_gain: float32 [512], replicated, may hold values from 0.1 to 1.9
- out_weight: bfloat16 [512, 2048], P(None, 'tp'), may hold values from -0.25 to 0.25
- out_gain: float32 [2048], replicated, may hold values from 0.1 to 1.9
- ffn_input: bfloat16 [1024, 2048], P('ep'), may hold values from -6 to 6
- ffn_gain: float32 [2048], replicated, may hold values from 0.1 to 1.9
- routes: int32 [1024, 4], P('ep'), may hold values from 0 to 7, all different within a row; in each aligned block of 128 rows (0 to 127, 128 to 255, ...) at most 128 rows name the same one
- route_weight: float32 [1024, 4], P('ep'), may hold values from 0.2 to 2
- gate_weight: bfloat16 [8, 2048, 4096], P('ep', None, 'tp'), may hold values from -0.375 to 0.375
- up_weight: bfloat16 [8, 2048, 4096], P('ep', None, 'tp'), may hold values from -0.375 to 0.375
- down_weight: bfloat16 [8, 4096, 2048], P('ep', 'tp'), may hold values from -0.0078125 to 0.0078125
Outputs:
- mixer_out: bfloat16 [8192, 2048], P(('ep', 'tp'))
- expert_out: bfloat16 [1024, 2048], P('ep', 'tp')
Inputs may be any that keep to these rules, and one draw needn't show every extreme that they name: `routes`: each row names 4 different experts. Among the 128 rows of one index of ep no expert is named by more than 128 rows, and in some such block one expert is named by exactly 128.
All inputs are finite; a program needn't handle non-finite values.
Results may differ from a plain program's by a relative error of at most 0.017.
Values may be sent and summed in bfloat16 or wider, within the bound.
A program may use at most 64 MiB of HBM per device.

v0:
```python
import jax
import jax.numpy as jnp
from jax import lax
from jax.sharding import PartitionSpec as P

pool_windows = (2, 4, 8, 16)
rim_rows = 15
norm_eps = 1e-06
clamp_limit = 7.0
sigmoid_slope = 1.702


def shifted_2(block, axis, distance):
    devices = range(lax.axis_size(axis))
    route = [(i - distance, i) for i in devices if i - distance in devices]
    return lax.ppermute(block, axis, route)


def rms_scale(values, gain):
    return values * lax.rsqrt(jnp.mean(values * values, axis=-1, keepdims=True) + norm_eps) * gain


def slot_tables(route_block, expert_count, capacity):
    row_count, top_count = route_block.shape
    flat_experts = route_block.reshape(-1)
    one_hot = (flat_experts[:, None] == jnp.arange(expert_count, dtype=jnp.int32)[None, :]).astype(
        jnp.int32
    )
    earlier = jnp.cumsum(one_hot, axis=0) - one_hot
    slot_index = jnp.sum(earlier * one_hot, axis=1)
    flat_slots = slot_index * expert_count + flat_experts
    owner_rows = jnp.full((capacity * expert_count,), row_count, jnp.int32)
    owner_rows = owner_rows.at[flat_slots].set(
        jnp.arange(row_count * top_count, dtype=jnp.int32) // top_count
    )
    return (flat_slots, owner_rows)


def pool_branch(branch_in, pool_weight, group_gain, out_weight, out_gain):
    row_count, width = branch_in.shape
    group_chans = width // len(pool_windows)
    rim = shifted_2(branch_in[row_count - rim_rows :], ("ep", "tp"), 1)
    widened = jnp.concatenate([rim, branch_in], axis=0).astype(jnp.float32)
    first_row = (lax.axis_index("ep") * lax.axis_size("tp") + lax.axis_index("tp")) * row_count
    positions = first_row + jnp.arange(row_count, dtype=jnp.int32)
    window = jnp.repeat(jnp.array(pool_windows, jnp.int32), group_chans)
    summed = jnp.zeros((row_count, width), jnp.float32)
    for offset_back in range(rim_rows + 1):
        shifted = widened[rim_rows - offset_back : rim_rows - offset_back + row_count]
        summed = summed + jnp.where(window[None, :] > offset_back, shifted, jnp.float32(0.0))
    counts = jnp.minimum(window[None, :], positions[:, None] + 1).astype(jnp.float32)
    pooled = (summed / counts - widened[rim_rows:]).astype(jnp.bfloat16)
    mixed_parts = []
    for group_index in range(len(pool_windows)):
        lower = group_index * group_chans
        mixed_parts.append(
            jnp.dot(
                pooled[:, lower : lower + group_chans],
                pool_weight[group_index],
                preferred_element_type=jnp.float32,
            )
        )
    group_mix = jnp.concatenate(mixed_parts, axis=1)
    mixed_rows = rms_scale(group_mix, group_gain).astype(jnp.bfloat16)
    projected = jnp.dot(
        mixed_rows,
        lax.all_gather(out_weight, "tp", axis=1, tiled=True),
        preferred_element_type=jnp.float32,
    )
    return rms_scale(projected, out_gain).astype(jnp.bfloat16)


def expert_hidden(slot_rows, gate_local, up_local):
    gate_pre = jnp.einsum("sed,df->sef", slot_rows, gate_local, preferred_element_type=jnp.float32)
    up_pre = jnp.einsum("sed,df->sef", slot_rows, up_local, preferred_element_type=jnp.float32)
    gate_pre = jnp.minimum(gate_pre, clamp_limit)
    up_pre = jnp.clip(up_pre, -clamp_limit, clamp_limit)
    return ((up_pre + 1.0) * gate_pre * jax.nn.sigmoid(sigmoid_slope * gate_pre)).astype(
        jnp.bfloat16
    )


def send_home(hidden, down_local):
    partial_sum = jnp.einsum("sef,fd->sed", hidden, down_local, preferred_element_type=jnp.float32)
    partial_sum = partial_sum.astype(jnp.bfloat16).astype(jnp.float32)
    summed = lax.psum_scatter(
        partial_sum.astype(jnp.bfloat16), "tp", scatter_dimension=2, tiled=True
    )
    return lax.all_to_all(summed, "ep", split_axis=1, concat_axis=1, tiled=True)


def per_device(
    branch_in,
    pool_weight,
    group_gain,
    out_weight,
    out_gain,
    ffn_input,
    ffn_gain,
    routes,
    route_weight,
    gate_weight,
    up_weight,
    down_weight,
):
    mixer_out = pool_branch(branch_in, pool_weight, group_gain, out_weight, out_gain)
    normed_rows = rms_scale(ffn_input.astype(jnp.float32), ffn_gain).astype(jnp.bfloat16)
    row_count, model_width = normed_rows.shape
    top_count = routes.shape[1]
    expert_count = lax.axis_size("ep")
    capacity = 2 * row_count * top_count // expert_count
    flat_slots, owner_rows = slot_tables(routes, expert_count, capacity)
    padded = jnp.concatenate([normed_rows, jnp.zeros((1, model_width), jnp.bfloat16)], axis=0)
    slot_rows = padded[owner_rows].reshape(capacity, expert_count, model_width)
    gate_local = gate_weight[0]
    up_local = up_weight[0]
    down_local = down_weight[0]
    share = capacity // lax.axis_size("tp")
    my_share = lax.dynamic_slice_in_dim(slot_rows, lax.axis_index("tp") * share, share, 0)
    arrived = lax.all_to_all(my_share, "ep", split_axis=1, concat_axis=1, tiled=True)
    hidden = expert_hidden(lax.all_gather(arrived, "tp", axis=0, tiled=True), gate_local, up_local)
    returned = send_home(hidden, down_local)
    column_count = returned.shape[2]
    picked = returned.reshape(capacity * expert_count, column_count)[flat_slots]
    picked = picked.reshape(row_count, top_count, column_count).astype(jnp.float32)
    expert_out = jnp.sum(picked * route_weight[:, :, None], axis=1).astype(jnp.bfloat16)
    return (mixer_out, expert_out)


def solution(mesh):
    in_specs = (
        P(("ep", "tp"), None),
        P(),
        P(),
        P(None, "tp"),
        P(),
        P("ep", None),
        P(),
        P("ep", None),
        P("ep", None),
        P("ep", None, "tp"),
        P("ep", None, "tp"),
        P("ep", "tp", None),
    )
    out_specs = (P(("ep", "tp"), None), P("ep", "tp"))
    return jax.shard_map(
        per_device, mesh=mesh, in_specs=in_specs, out_specs=out_specs, check_vma=False
    )
```

profile of v0, /device:TPU:0, one launch (start us, length us, event | category | flops | bytes accessed | tf_op | source)
XLA Modules:
  0.0 230.9 jit_solution(12385050998380482686)
XLA Ops:
  7.2 0.8 copy.16
  8.4 1.1 reduce-window.6
  9.5 0.2 slice_reduce_fusion
  9.9 2.4 %scatter_custom_fusion = s32[1024]{0:T(1024)S(1)} fusion(s32[512]{0:T(512)S(1)} %bitcast.66, s32[512]{0:T(512)S(1)} %add_select_fusion, s32[]{:T(128)} %constant.34.clone.1), kind=kCustom, calls=%fused_computation.109 | custom fusion | bytes 4100 | tf_op jit(solution)/shard_map/scatter | solution.py:33
  12.3 1.2 fusion.11
  13.6 1.2 fusion.13
  14.9 6.0 %gather_fusion = bf16[1024,2048]{1,0:T(8,128)(2,1)} fusion(bf16[129,2048]{1,0:T(8,128)(2,1)S(1)} %concatenate.11, s32[1024]{0:T(1024)S(1)} %fusion.54), kind=kCustom, calls=%fused_computation | custom fusion | bytes 8392704 | tf_op jit(solution)/shard_map/gather | solution.py:114
  20.9 1.3 constant_dynamic-slice_fusion
  22.2 0.6 copy.22
  22.8 32.8 %all_to_all.10 = bf16[32,8,2048]{2,0,1:T(8,128)(2,1)} all-to-all(bf16[32,8,2048]{2,0,1:T(8,128)(2,1)S(1)} %copy.22), channel_id=1, replica_groups=mesh['ep'=8,'tp'=4] {'ep'}, dimensions={1} | all-to-all | bytes 2097152 | tf_op jit(solution)/shard_map/all_to_all | solution.py:120
  55.7 51.6 %all-gather.5.cloned.1.call-done = bf16[128,8,2048]{2,0,1:T(8,128)(2,1)} async-done(((bf16[32,8,2048]{2,0,1:T(8,128)(2,1)}), bf16[128,8,2048]{2,0,1:T(8,128)(2,1)}) %all-gather.5.cloned.1.call-update) | async-done | bytes 4194320 | tf_op jit(solution)/shard_map/all_gather | solution.py:121
  107.3 7.6 %fusion.2 = f32[128,8,1024]{2,0,1:T(8,128)S(1)} fusion(bf16[128,8,2048]{2,0,1:T(8,128)(2,1)} %all-gather.5.cloned.1.call-done, bf16[1,2048,1024]{2,1,0:T(8,128)(2,1)} %param.22), kind=kOutput, calls=%fused_computation.5 | convolution fusion | flops 4294967296 | bytes 12582912 | tf_op jit(solution)/shard_map/sed,df->sef/dot_general | solution.py:74
  115.0 5.7 %multiply_convert_fusion = bf16[128,8,1024]{2,0,1:T(8,128)(2,1)S(1)} fusion(f32[128,8,1024]{2,0,1:T(8,128)S(1)} %fusion.2, bf16[128,8,2048]{2,0,1:T(8,128)(2,1)S(1)} %copy-done.8, bf16[1,2048,1024]{2,1,0:T(8,128)(2,1)S(1)} %copy-done.6), kind=kOutput, calls=%fused_computation.9 | convolution fusion | flops 4305453056 | bytes 14680064 | tf_op jit(solution)/shard_map/sed,df->sef/dot_general | solution.py:75
  120.6 6.1 %fusion.6 = bf16[128,8,2048]{2,0,1:T(8,128)(2,1)} fusion(bf16[128,8,1024]{2,0,1:T(8,128)(2,1)S(1)} %multiply_convert_fusion, bf16[1,1024,2048]{2,1,0:T(8,128)(2,1)S(1)} %copy-done.7), kind=kOutput, calls=%fused_computation.10 | convolution fusion | flops 4297064448 | bytes 10485760 | tf_op jit(solution)/shard_map/sef,fd->sed/dot_general | solution.py:84
  126.8 0.7 all-gather.3.cloned.1.call-update
  127.5 0.2 copy-done
  127.7 3.4 %collective-permute-start = (bf16[15,512]{1,0:T(8,128)(2,1)S(1)}, bf16[15,512]{1,0:T(8,128)(2,1)S(1)}, u32[]{:S(2)}, u32[]{:S(2)}) collective-permute-start(bf16[15,512]{1,0:T(8,128)(2,1)S(1)} %slice.82), channel_id=1, source_target_pairs={{0,1},{1,2},{2,3},{3,4},{4,5},{5,6},{6,7},{7,8},{8,9},{9,10},{10,1... | collective-permute-start | bytes 46088 | tf_op jit(solution)/shard_map/ppermute | solution.py:16
  131.4 1.1 collective-permute-done
  132.6 1.1 fusion.31
  133.8 0.2 fusion.35
  134.0 45.5 %reduce-scatter.2.cloned.1.call-done = bf16[128,8,512]{2,0,1:T(8,128)(2,1)} async-done(((bf16[128,8,2048]{2,0,1:T(8,128)(2,1)}), bf16[128,8,512]{2,0,1:T(8,128)(2,1)}) %reduce-scatter.2.cloned.1.call-update) | async-done | bytes 1048592 | tf_op jit(solution)/shard_map/reduce_scatter | solution.py:86
  179.5 4.6 %all-to-all-start.1 = ((bf16[128,8,512]{2,0,1:T(8,128)(2,1)}), bf16[128,8,512]{2,0,1:T(8,128)(2,1)S(1)}, u32[]{:S(2)}, u32[]{:S(2)}) async-start(bf16[128,8,512]{2,0,1:T(8,128)(2,1)} %reduce-scatter.2.cloned.1.call-done), calls=%async_computation.2 | async-start | bytes 2097152 | tf_op jit(solution)/shard_map/all_to_all | solution.py:89
  184.1 0.2 fusion.37
  184.3 0.2 fusion.39
  184.5 0.2 fusion.41
  184.8 31.5 %all-gather.3.cloned.1.call-done = bf16[512,2048]{1,0:T(8,128)(2,1)} async-done(((bf16[512,512]{1,0:T(8,128)(2,1)}), bf16[512,2048]{1,0:T(8,128)(2,1)}) %all-gather.3.cloned.1.call-update) | async-done | bytes 2097168 | tf_op jit(solution)/shard_map/all_gather | solution.py:67
  216.4 2.5 %multiply_reduce_fusion = (f32[256]{0:T(256)S(1)}, f32[256,2048]{1,0:T(8,128)S(1)}) fusion(bf16[512,2048]{1,0:T(8,128)(2,1)} %all-gather.3.cloned.1.call-done, f32[256,128]{0,1:T(8,128)S(1)} %fusion.35, f32[256,128]{0,1:T(8,128)S(1)} %fusion.37, f32[256,128]{0,1:T(8,128)S(1)} %fusion.39, f32[256,128]{0,1:T(8,128)S(1)} %fusion.41, f32[512]{0:T(512)S(1)} %copy-done.3, ...), kind=kOutput, calls=%fused_computation.12 | convolution fusion | flops 538705664 | bytes 4722688 | tf_op jit(solution)/shard_map/dot_general | solution.py:65
  218.9 1.2 multiply_convert_fusion.1
  220.2 0.6 copy.24
  220.7 2.0 gather_fusion.1
  222.7 0.3 reshape.212
  223.0 1.4 multiply_reduce_fusion.1
  (46 shorter events, 1.2 us)
Async XLA Ops:
  7.2 100.1 %all-gather.5.cloned.1.call-start = ((), (), s32[]{:S(2)}) async-start(), calls=%async_computation.4 | async-start | bytes 5242880 | tf_op jit(solution)/shard_map/all_gather | solution.py:121
  55.6 123.9 %reduce-scatter.2.cloned.1.call-start = ((), (), s32[]{:S(2)}) async-start(), calls=%async_computation.5 | async-start | bytes 5242880 | tf_op jit(solution)/shard_map/reduce_scatter | solution.py:86
  107.3 7.7 %copy-start.6 = (bf16[1,2048,1024]{2,1,0:T(8,128)(2,1)S(1)}, bf16[1,2048,1024]{2,1,0:T(8,128)(2,1)}, u32[]{:S(2)}) copy-start(bf16[1,2048,1024]{2,1,0:T(8,128)(2,1)} %param.23) | copy-start | bytes 12582916
  107.3 7.7 %copy-start.8 = (bf16[128,8,2048]{2,0,1:T(8,128)(2,1)S(1)}, bf16[128,8,2048]{2,0,1:T(8,128)(2,1)}, u32[]{:S(2)}) copy-start(bf16[128,8,2048]{2,0,1:T(8,128)(2,1)} %all-gather.5.cloned.1.call-done) | copy-start | bytes 12582916
  115.0 5.7 %copy-start.7 = (bf16[1,1024,2048]{2,1,0:T(8,128)(2,1)S(1)}, bf16[1,1024,2048]{2,1,0:T(8,128)(2,1)}, u32[]{:S(2)}) copy-start(bf16[1,1024,2048]{2,1,0:T(8,128)(2,1)} %param.24) | copy-start | bytes 12582916
  126.7 0.9 copy-start
  126.7 4.4 %copy-start.5 = (s32[4]{0:T(128)S(1)}, s32[4]{0:T(128)}, u32[]{:S(2)}) copy-start(s32[4]{0:T(128)} %constant.101.clone) | copy-start | bytes 52
  126.7 4.5 %copy-start.4 = (f32[128,4]{0,1:T(4,128)S(1)}, f32[128,4]{0,1:T(4,128)}, u32[]{:S(2)}) copy-start(f32[128,4]{0,1:T(4,128)} %param.21) | copy-start | bytes 6148
  126.7 89.6 %all-gather.3.cloned.1.call-start = ((), (), s32[]{:S(2)}) async-start(), calls=%async_computation.3 | async-start | bytes 2621440 | tf_op jit(solution)/shard_map/all_gather | solution.py:67
  127.7 4.8 %collective-permute-start = (bf16[15,512]{1,0:T(8,128)(2,1)S(1)}, bf16[15,512]{1,0:T(8,128)(2,1)S(1)}, u32[]{:S(2)}, u32[]{:S(2)}) collective-permute-start(bf16[15,512]{1,0:T(8,128)(2,1)S(1)} %slice.82), channel_id=1, source_target_pairs={{0,1},{1,2},{2,3},{3,4},{4,5},{5,6},{6,7},{7,8},{8,9},{9,10},{10,1... | collective-permute-start | bytes 46088 | tf_op jit(solution)/shard_map/ppermute | solution.py:16
  132.6 1.2 copy-start.1
  132.6 83.8 %copy-start.3 = (f32[512]{0:T(512)S(1)}, f32[512]{0:T(512)}, u32[]{:S(2)}) copy-start(f32[512]{0:T(512)} %param.15) | copy-start | bytes 6148
  133.7 85.2 %copy-start.2 = (f32[2048]{0:T(1024)S(1)}, f32[2048]{0:T(1024)}, u32[]{:S(2)}) copy-start(f32[2048]{0:T(1024)} %param.17) | copy-start | bytes 24580
  179.5 40.7 %all-to-all-start.1 = ((bf16[128,8,512]{2,0,1:T(8,128)(2,1)}), bf16[128,8,512]{2,0,1:T(8,128)(2,1)S(1)}, u32[]{:S(2)}, u32[]{:S(2)}) async-start(bf16[128,8,512]{2,0,1:T(8,128)(2,1)} %reduce-scatter.2.cloned.1.call-done), calls=%async_computation.2 | async-start | bytes 2097152 | tf_op jit(solution)/shard_map/all_to_all | solution.py:89
Sparse Core Ops, SparseCore 0:
  55.7 51.4 all-gather.4
  126.9 52.5 reduce-scatter.1
  181.3 35.0 all-gather.2
where the time goes:
time: 231 us
  waiting for transfers between devices  130 us (56%)
  blocking collectives  32.8 us (14%)
  matrix products  22.7 us (10%)
  local copies, waits for them, and re-layouts  15 us (6%)
  between operations  14 us (6%)
  starting transfers between devices  8.11 us (4%)
  other arithmetic  7.78 us (3%)
    all_gather x1, waiting for transfers between devices, per_device(): lax.all_gather(arrived, 'tp', axis=0, tiled=True)  51.6 us
    reduce_scatter x1, waiting for transfers between devices, send_home(): lax.psum_scatter(partial_sum.astype(jnp.bfloat16), 'tp', scatter_dimensio...  45.5 us
    all_to_all x1, blocking collectives, per_device(): lax.all_to_all(my_share, 'ep', split_axis=1, concat_axis=1, tiled=True)  32.8 us
    all_gather x1, waiting for transfers between devices, pool_branch(): lax.all_gather(out_weight, 'tp', axis=1, tiled=True)  31.5 us
    dot_general x1, matrix products, expert_hidden(): jnp.einsum('sed,df->sef', slot_rows, gate_local, preferred_element_type=j...  7.64 us
    dot_general x1, matrix products, send_home(): jnp.einsum('sef,fd->sed', hidden, down_local, preferred_element_type=jnp....  6.07 us
    gather x1, local copies, waits for them, and re-layouts, per_device(): slot_rows = padded[owner_rows].reshape(capacity, expert_count, model_width)  6.02 us
    dot_general x1, matrix products, expert_hidden(): jnp.einsum('sed,df->sef', slot_rows, up_local, preferred_element_type=jnp...  5.65 us
  transfers between devices with their start and end apart: 5, of which 4 were waited for; matrix products, arithmetic and copies ran while one was open for 3% of the time, Pallas kernels for 0%

commit v1 on v0

--- a/solution.py
+++ b/solution.py
@@ -117,7 +117,10 @@
     down_local = down_weight[0]
     share = capacity // lax.axis_size("tp")
     my_share = lax.dynamic_slice_in_dim(slot_rows, lax.axis_index("tp") * share, share, 0)
-    arrived = lax.all_to_all(my_share, "ep", split_axis=1, concat_axis=1, tiled=True)
+    arrived = jnp.concatenate(
+        lax.all_to_all(jnp.stack(jnp.split(my_share, lax.axis_size("ep"), axis=1)), "ep", 0, 0),
+        axis=1,
+    )
     hidden = expert_hidden(lax.all_gather(arrived, "tp", axis=0, tiled=True), gate_local, up_local)
     returned = send_home(hidden, down_local)
     column_count = returned.shape[2]

time: 231 us -> 243 us (1.052)
  matrix products: 22.7 us -> 29.2 us
  local copies, waits for them, and re-layouts: 15 us -> 20.8 us
    dot_general x1, matrix products: 6.07 us -> 15.9 us  [send_home(): jnp.einsum('sef,fd->sed', hidden, down_local, preferred_element_type=jnp....]
    split x0 -> x1, local copies, waits for them, and re-layouts: none -> 6.99 us  [per_device(): jnp.split(my_share, lax.axis_size('ep'), axis=1)]
    dot_general x1 -> x0, matrix products: 5.65 us -> none  [expert_hidden(): jnp.einsum('sed,df->sef', slot_rows, up_local, preferred_element_type=jnp...]
where the time goes in v1:
time: 243 us
  waiting for transfers between devices  130 us (53%)
  blocking collectives  32.8 us (13%)
  matrix products  29.2 us (12%)
  local copies, waits for them, and re-layouts  20.8 us (9%)
  between operations  14 us (6%)
  starting transfers between devices  8.26 us (3%)
  other arithmetic  7.78 us (3%)
    all_gather x1, waiting for transfers between devices, per_device(): lax.all_gather(arrived, 'tp', axis=0, tiled=True)  51.3 us
    reduce_scatter x1, waiting for transfers between devices, send_home(): lax.psum_scatter(partial_sum.astype(jnp.bfloat16), 'tp', scatter_dimensio...  45.6 us
    all_to_all x1, blocking collectives, per_device(): lax.all_to_all(jnp.stack(jnp.split(my_share, lax.axis_size('ep'), axis=1)...  32.8 us
    all_gather x1, waiting for transfers between devices, pool_branch(): lax.all_gather(out_weight, 'tp', axis=1, tiled=True)  31.6 us
    dot_general x1, matrix products, send_home(): jnp.einsum('sef,fd->sed', hidden, down_local, preferred_element_type=jnp....  15.9 us
    dot_general x1, matrix products, expert_hidden(): jnp.einsum('sed,df->sef', slot_rows, gate_local, preferred_element_type=j...  9.93 us
    split x1, local copies, waits for them, and re-layouts, per_device(): jnp.split(my_share, lax.axis_size('ep'), axis=1)  6.99 us
    gather x1, local copies, waits for them, and re-layouts, per_device(): slot_rows = padded[owner_rows].reshape(capacity, expert_count, model_width)  6.02 us
  transfers between devices with their start and end apart: 5, of which 4 were waited for; matrix products, arithmetic and copies ran while one was open for 3% of the time, Pallas kernels for 0%

profile of v1, /device:TPU:0, one launch (start us, length us, event | category | flops | bytes accessed | tf_op | source)
XLA Modules:
  0.0 243.0 jit_solution(16158029660392935601)
XLA Ops:
  7.2 0.8 copy.112
  8.4 1.1 reduce-window.6
  9.5 0.2 slice_reduce_fusion
  9.9 2.4 %scatter_custom_fusion = s32[1024]{0:T(1024)S(1)} fusion(s32[512]{0:T(512)S(1)} %bitcast.94, s32[512]{0:T(512)S(1)} %add_select_fusion, s32[]{:T(128)} %constant.34.clone.1), kind=kCustom, calls=%fused_computation.123 | custom fusion | bytes 4100 | tf_op jit(solution)/shard_map/scatter | solution.py:33
  12.3 1.2 fusion.23
  13.6 1.2 fusion.25
  14.9 6.0 %gather_fusion = bf16[1024,2048]{1,0:T(8,128)(2,1)} fusion(bf16[129,2048]{1,0:T(8,128)(2,1)S(1)} %concatenate.11, s32[1024]{0:T(1024)S(1)} %fusion.66), kind=kCustom, calls=%fused_computation | custom fusion | bytes 8392704 | tf_op jit(solution)/shard_map/gather | solution.py:114
  20.9 7.0 %constant_dynamic-slice_fusion.7 = (bf16[32,1,2048]{2,1,0:T(2,128)(2,1)S(1)}, bf16[32,1,2048]{2,1,0:T(2,128)(2,1)S(1)}, bf16[32,1,2048]{2,1,0:T(2,128)(2,1)S(1)}...) fusion(bf16[128,8,2048]{2,1,0:T(8,128)(2,1)} %bitcast.92, ...), kind=kLoop, calls=%fused_computation.132 | loop fusion | bytes 2097184 | tf_op jit(solution)/shard_map/split | solution.py:121
  28.6 32.8 %all_to_all.10 = bf16[8,32,1,2048]{3,1,2,0:T(8,128)(2,1)} all-to-all(bf16[8,32,1,2048]{3,1,2,0:T(8,128)(2,1)S(1)} %bitcast_dynamic-update-slice_fusion), channel_id=1, replica_groups=mesh['ep'=8,'tp'=4] {'ep'}, dimensions={0} | all-to-all | bytes 2097152 | tf_op jit(solution)/shard_map/all_to_all | solution.py:121
  61.5 0.2 reduce-scatter.2.cloned.1.call-start
  61.7 51.3 %all-gather.6.cloned.1.call-done = bf16[128,8,1,2048]{3,0,1,2:T(8,128)(2,1)} async-done(((bf16[32,8,1,2048]{3,0,1,2:T(8,128)(2,1)}), bf16[128,8,1,2048]{3,0,1,2:T(8,128)(2,1)}) %all-gather.6.cloned.1.call-update) | async-done | bytes 4194320 | tf_op jit(solution)/shard_map/all_gather | solution.py:124
  113.0 9.9 %fusion.2 = f32[128,8,1024]{2,0,1:T(8,128)} fusion(bf16[1,2048,1024]{2,1,0:T(8,128)(2,1)} %param.22, bf16[128,8,1,2048]{3,0,1,2:T(8,128)(2,1)} %all-gather.6.cloned.1.call-done), kind=kOutput, calls=%fused_computation.5 | convolution fusion | flops 4294967296 | bytes 12582912 | tf_op jit(solution)/shard_map/sed,df->sef/dot_general | solution.py:74
  122.9 15.9 %fusion.8 = bf16[128,8,2048]{2,0,1:T(8,128)(2,1)} fusion(bf16[1,1024,2048]{2,1,0:T(8,128)(2,1)} %param.24, f32[128,8,1024]{2,0,1:T(8,128)} %fusion.2, bf16[1,2048,1024]{2,1,0:T(8,128)(2,1)} %param.23, bf16[128,8,1,2048]{3,0,1,2:T(8,128)(2,1)} %all-gather.6.cloned.1.call-done), kind=kOutput, calls=%fused_computation.12 | convolution fusion | flops 8602517504 | bytes 20971520 | tf_op jit(solution)/shard_map/sef,fd->sed/dot_general | solution.py:84
  138.9 0.7 all-gather.4.cloned.1.call-update
  139.5 0.2 copy-done
  139.7 3.4 %collective-permute-start = (bf16[15,512]{1,0:T(8,128)(2,1)S(1)}, bf16[15,512]{1,0:T(8,128)(2,1)S(1)}, u32[]{:S(2)}, u32[]{:S(2)}) collective-permute-start(bf16[15,512]{1,0:T(8,128)(2,1)S(1)} %slice.82), channel_id=1, source_target_pairs={{0,1},{1,2},{2,3},{3,4},{4,5},{5,6},{6,7},{7,8},{8,9},{9,10},{10,1... | collective-permute-start | bytes 46088 | tf_op jit(solution)/shard_map/ppermute | solution.py:16
  143.3 0.1 copy.117
  143.4 1.1 collective-permute-done
  144.6 1.1 fusion.43
  145.8 0.2 fusion.47
  146.0 45.6 %reduce-scatter.2.cloned.1.call-done = bf16[128,8,512]{2,0,1:T(8,128)(2,1)} async-done(((bf16[128,8,2048]{2,0,1:T(8,128)(2,1)}), bf16[128,8,512]{2,0,1:T(8,128)(2,1)}) %reduce-scatter.2.cloned.1.call-update) | async-done | bytes 1048592 | tf_op jit(solution)/shard_map/reduce_scatter | solution.py:86
  191.6 4.6 %all-to-all-start.1 = ((bf16[128,8,512]{2,0,1:T(8,128)(2,1)}), bf16[128,8,512]{2,0,1:T(8,128)(2,1)S(1)}, u32[]{:S(2)}, u32[]{:S(2)}) async-start(bf16[128,8,512]{2,0,1:T(8,128)(2,1)} %reduce-scatter.2.cloned.1.call-done), calls=%async_computation.2 | async-start | bytes 2097152 | tf_op jit(solution)/shard_map/all_to_all | solution.py:89
  196.2 0.2 fusion.49
  196.4 0.2 fusion.51
  196.6 0.2 fusion.53
  196.9 31.6 %all-gather.4.cloned.1.call-done = bf16[512,2048]{1,0:T(8,128)(2,1)} async-done(((bf16[512,512]{1,0:T(8,128)(2,1)}), bf16[512,2048]{1,0:T(8,128)(2,1)}) %all-gather.4.cloned.1.call-update) | async-done | bytes 2097168 | tf_op jit(solution)/shard_map/all_gather | solution.py:67
  228.5 2.5 %multiply_reduce_fusion = (f32[256]{0:T(256)S(1)}, f32[256,2048]{1,0:T(8,128)S(1)}) fusion(bf16[512,2048]{1,0:T(8,128)(2,1)} %all-gather.4.cloned.1.call-done, f32[256,128]{0,1:T(8,128)S(1)} %fusion.47, f32[256,128]{0,1:T(8,128)S(1)} %fusion.49, f32[256,128]{0,1:T(8,128)S(1)} %fusion.51, f32[256,128]{0,1:T(8,128)S(1)} %fusion.53, f32[512]{0:T(512)S(1)} %copy-done.3, ...), kind=kOutput, calls=%fused_computation.18 | convolution fusion | flops 538705664 | bytes 4722688 | tf_op jit(solution)/shard_map/dot_general | solution.py:65
  231.0 1.2 multiply_convert_fusion.1
  232.2 0.6 copy.135
  232.8 2.0 gather_fusion.1
  234.8 0.3 reshape.220
  235.1 1.4 multiply_reduce_fusion.1
  (46 shorter events, 1.7 us)
Async XLA Ops:
  7.2 105.8 %all-gather.6.cloned.1.call-start = ((), (), s32[]{:S(2)}) async-start(), calls=%async_computation.5 | async-start | bytes 5242880 | tf_op jit(solution)/shard_map/all_gather | solution.py:124
  61.5 130.1 %reduce-scatter.2.cloned.1.call-start = ((), (), s32[]{:S(2)}) async-start(), calls=%async_computation.4 | async-start | bytes 5242880 | tf_op jit(solution)/shard_map/reduce_scatter | solution.py:86
  138.8 0.9 copy-start
  138.8 4.3 %copy-start.5 = (s32[4]{0:T(128)S(1)}, s32[4]{0:T(128)}, u32[]{:S(2)}) copy-start(s32[4]{0:T(128)} %constant.101.clone) | copy-start | bytes 52
  138.8 4.5 %copy-start.4 = (f32[128,4]{0,1:T(4,128)S(1)}, f32[128,4]{0,1:T(4,128)}, u32[]{:S(2)}) copy-start(f32[128,4]{0,1:T(4,128)} %param.21) | copy-start | bytes 6148
  138.8 89.7 %all-gather.4.cloned.1.call-start = ((), (), s32[]{:S(2)}) async-start(), calls=%async_computation.3 | async-start | bytes 2621440 | tf_op jit(solution)/shard_map/all_gather | solution.py:67
  139.7 4.8 %collective-permute-start = (bf16[15,512]{1,0:T(8,128)(2,1)S(1)}, bf16[15,512]{1,0:T(8,128)(2,1)S(1)}, u32[]{:S(2)}, u32[]{:S(2)}) collective-permute-start(bf16[15,512]{1,0:T(8,128)(2,1)S(1)} %slice.82), channel_id=1, source_target_pairs={{0,1},{1,2},{2,3},{3,4},{4,5},{5,6},{6,7},{7,8},{8,9},{9,10},{10,1... | collective-permute-start | bytes 46088 | tf_op jit(solution)/shard_map/ppermute | solution.py:16
  144.6 1.2 copy-start.1
  144.6 83.9 %copy-start.3 = (f32[512]{0:T(512)S(1)}, f32[512]{0:T(512)}, u32[]{:S(2)}) copy-start(f32[512]{0:T(512)} %param.15) | copy-start | bytes 6148
  145.8 85.2 %copy-start.2 = (f32[2048]{0:T(1024)S(1)}, f32[2048]{0:T(1024)}, u32[]{:S(2)}) copy-start(f32[2048]{0:T(1024)} %param.17) | copy-start | bytes 24580
  191.6 40.7 %all-to-all-start.1 = ((bf16[128,8,512]{2,0,1:T(8,128)(2,1)}), bf16[128,8,512]{2,0,1:T(8,128)(2,1)S(1)}, u32[]{:S(2)}, u32[]{:S(2)}) async-start(bf16[128,8,512]{2,0,1:T(8,128)(2,1)} %reduce-scatter.2.cloned.1.call-done), calls=%async_computation.2 | async-start | bytes 2097152 | tf_op jit(solution)/shard_map/all_to_all | solution.py:89
Sparse Core Ops, SparseCore 0:
  61.6 51.3 all-gather.5
  138.9 52.5 reduce-scatter.1
  193.4 35.0 all-gather.3
